TPU v7x, 32 devices: a whole 2x2x4 slice. The times are simulated.
32 devices in a mesh: fs: 8 (over z, x), tp: 4 (over y, core).
Axes of the slice: x: 2, y: 2, z: 4, core: 2. Of those that a mesh axis runs over, the one named last changes fastest.
Arguments:
- tokens: bfloat16 [4096, 2048], P(('fs', 'tp')), may hold values from -6 to 6
- gate_weight: bfloat16 [5632, 2048], P('tp', 'fs'), may hold values from -0.125 to 0.125
- up_weight: bfloat16 [5632, 2048], P('tp', 'fs'), may hold values from -0.125 to 0.125
- down_weight: bfloat16 [5632, 2048], P('tp', 'fs'), may hold values from -0.078125 to 0.078125
- out_grad: bfloat16 [4096, 2048], P(('fs', 'tp')), may hold values from -6 to 6
Outputs:
- grad_tokens: bfloat16 [4096, 2048], P(('fs', 'tp'))
- grad_gate: float32 [5632, 2048], P('tp', 'fs')
- grad_up: float32 [5632, 2048], P('tp', 'fs')
- grad_down: float32 [5632, 2048], P('tp', 'fs')
- gate_rows: float32 [5632], P('tp')
- up_rows: float32 [5632], P('tp')
- down_rows: float32 [5632], P('tp')
All inputs are finite; a program needn't handle non-finite values.
Results may differ from a plain program's by a relative error of at most 0.014.
Values may be sent and summed in bfloat16 or wider, within the bound.
A program may use at most 128 MiB of HBM per device.

v0:
```python
import math
import jax
import jax.numpy as jnp
from jax import lax
from jax.sharding import PartitionSpec as P


def body(tokens, gate_weight, up_weight, down_weight, out_grad):
    inputs, cotangent = (
        lax.all_gather(tokens, "tp", axis=0, tiled=True),
        lax.all_gather(out_grad, "tp", axis=0, tiled=True),
    )
    w_gate, w_up, w_down = (
        lax.all_gather(gate_weight, "fs", axis=1, tiled=True),
        lax.all_gather(up_weight, "fs", axis=1, tiled=True),
        lax.all_gather(down_weight, "fs", axis=1, tiled=True),
    )
    inner = (((1,), (1,)), ((), ()))
    gate = lax.dot_general(inputs, w_gate, inner, preferred_element_type=jnp.float32)
    up = lax.dot_general(inputs, w_up, inner, preferred_element_type=jnp.float32)
    dhidden = lax.dot_general(cotangent, w_down, inner, preferred_element_type=jnp.float32)
    sig = jax.nn.sigmoid(gate)
    silu = gate * sig
    act = (silu * up).astype(jnp.bfloat16)
    dgate = (dhidden * up * sig * (1.0 + gate * (1.0 - sig))).astype(jnp.bfloat16)
    dup = (dhidden * silu).astype(jnp.bfloat16)
    term = jnp.dot(dgate, w_gate, preferred_element_type=jnp.float32)
    grad_tokens = lax.psum_scatter(
        (term + jnp.dot(dup, w_up, preferred_element_type=jnp.float32)).astype(jnp.bfloat16),
        "tp",
        scatter_dimension=0,
        tiled=True,
    )
    factor = 1.0 / math.sqrt(inputs.shape[0] * lax.axis_size("fs"))
    outer = (((0,), (0,)), ((), ()))
    width = gate_weight.shape[1] * lax.axis_size("fs")
    part_gate = lax.dot_general(dgate, inputs, outer, preferred_element_type=jnp.float32) * factor
    part_up = lax.dot_general(dup, inputs, outer, preferred_element_type=jnp.float32) * factor
    part_down = lax.dot_general(act, cotangent, outer, preferred_element_type=jnp.float32) * factor
    grad_gate, grad_up, grad_down = (
        lax.psum_scatter(
            part_gate.astype(jnp.bfloat16), "fs", scatter_dimension=1, tiled=True
        ).astype(jnp.float32),
        lax.psum_scatter(
            part_up.astype(jnp.bfloat16), "fs", scatter_dimension=1, tiled=True
        ).astype(jnp.float32),
        lax.psum_scatter(
            part_down.astype(jnp.bfloat16), "fs", scatter_dimension=1, tiled=True
        ).astype(jnp.float32),
    )
    sums = lax.psum(
        (
            jnp.sum(grad_gate * grad_gate, axis=1),
            jnp.sum(grad_up * grad_up, axis=1),
            jnp.sum(grad_down * grad_down, axis=1),
        ),
        "fs",
    )
    gate_rows, up_rows, down_rows = (sums[0] / width, sums[1] / width, sums[2] / width)
    return (grad_tokens, grad_gate, grad_up, grad_down, gate_rows, up_rows, down_rows)


def solution(mesh):
    return jax.shard_map(
        body,
        mesh=mesh,
        in_specs=(
            P(("fs", "tp"), None),
            P("tp", "fs"),
            P("tp", "fs"),
            P("tp", "fs"),
            P(("fs", "tp"), None),
        ),
        out_specs=(
            P(("fs", "tp"), None),
            P("tp", "fs"),
            P("tp", "fs"),
            P("tp", "fs"),
            P("tp"),
            P("tp"),
            P("tp"),
        ),
        check_vma=False,
    )
```

profile of v0, /device:TPU:0, one launch (start us, length us, event | category | flops | bytes accessed | tf_op | source)
XLA Modules:
  0.0 727.2 jit_solution(359217630501200977)
XLA Ops:
  7.2 0.7 all-gather.10.cloned.1.call-update
  7.9 0.7 all-gather.12.cloned.1.call-update
  8.7 0.7 all-gather.14.cloned.1.call-update
  10.6 24.3 %all-gather.10.cloned.1.call-done = bf16[512,2048]{1,0:T(8,128)(2,1)} async-done(((bf16[128,2048]{1,0:T(8,128)(2,1)}), bf16[512,2048]{1,0:T(8,128)(2,1)}) %all-gather.10.cloned.1.call-update) | async-done | bytes 2097168 | tf_op jit(solution)/shard_map/all_gather | solution.py:10
  34.9 95.2 %all-gather.12.cloned.1.call-done = bf16[1408,2048]{1,0:T(8,128)(2,1)} async-done(((bf16[1408,256]{1,0:T(8,128)(2,1)}), bf16[1408,2048]{1,0:T(8,128)(2,1)}) %all-gather.12.cloned.1.call-update) | async-done | bytes 5767184 | tf_op jit(solution)/shard_map/all_gather | solution.py:15
  130.1 8.3 %fusion.3 = f32[512,1408]{1,0:T(8,128)} fusion(bf16[512,2048]{1,0:T(8,128)(2,1)} %all-gather.10.cloned.1.call-done, bf16[1408,2048]{1,0:T(8,128)(2,1)} %all-gather.12.cloned.1.call-done), kind=kOutput, calls=%fused_computation.16 | convolution fusion | flops 2952790016 | bytes 10747904 | tf_op jit(solution)/shard_map/dot_general | solution.py:20
  138.4 85.1 %all-gather.14.cloned.1.call-done = bf16[1408,2048]{1,0:T(8,128)(2,1)} async-done(((bf16[1408,256]{1,0:T(8,128)(2,1)}), bf16[1408,2048]{1,0:T(8,128)(2,1)}) %all-gather.14.cloned.1.call-update) | async-done | bytes 5767184 | tf_op jit(solution)/shard_map/all_gather | solution.py:14
  223.5 7.6 %fusion.4 = f32[512,1408]{1,0:T(8,128)} fusion(bf16[512,2048]{1,0:T(8,128)(2,1)S(1)} %copy-done, bf16[1408,2048]{1,0:T(8,128)(2,1)} %all-gather.14.cloned.1.call-done), kind=kOutput, calls=%fused_computation.17 | convolution fusion | flops 2952790016 | bytes 10747904 | tf_op jit(solution)/shard_map/dot_general | solution.py:19
  231.1 14.6 %all-gather.6.cloned.1.call-done = bf16[512,2048]{1,0:T(8,128)(2,1)} async-done(((bf16[128,2048]{1,0:T(8,128)(2,1)}), bf16[512,2048]{1,0:T(8,128)(2,1)}) %all-gather.6.cloned.1.call-update) | async-done | bytes 2097168 | tf_op jit(solution)/shard_map/all_gather | solution.py:11
  245.7 9.1 %multiply_convert_fusion = bf16[1408,2048]{1,0:T(8,128)(2,1)} fusion(bf16[512,2048]{1,0:T(8,128)(2,1)} %all-gather.6.cloned.1.call-done, f32[512,1408]{1,0:T(8,128)} %fusion.3, f32[512,1408]{1,0:T(8,128)} %fusion.4), kind=kOutput, calls=%fused_computation | convolution fusion | flops 2962882560 | bytes 13631488 | tf_op jit(solution)/shard_map/dot_general | solution.py:39
  255.0 85.7 %all-gather.8.cloned.1.call-done = bf16[1408,2048]{1,0:T(8,128)(2,1)} async-done(((bf16[1408,256]{1,0:T(8,128)(2,1)}), bf16[1408,2048]{1,0:T(8,128)(2,1)}) %all-gather.8.cloned.1.call-update) | async-done | bytes 5767184 | tf_op jit(solution)/shard_map/all_gather | solution.py:16
  340.7 10.2 %multiply_convert_fusion.4 = (bf16[512,1408]{1,0:T(8,128)(2,1)S(1)}, bf16[512,1408]{1,0:T(8,128)(2,1)}) fusion(f32[512,1408]{1,0:T(8,128)} %fusion.4, f32[512,1408]{1,0:T(8,128)} %fusion.3, bf16[512,2048]{1,0:T(8,128)(2,1)} %all-gather.6.cloned.1.call-done, bf16[1408,2048]{1,0:T(8,128)(2,1)} %all-gather.8.cloned.1.call-done), kind=kOutput, calls=%fused_computation.5 | convolution fusion | flops 2962161664 | bytes 16515072 | tf_op jit(solution)/shard_map/dot_general | solution.py:21
  350.9 5.0 multiply_convert_fusion.1
  355.9 6.5 multiply_convert_fusion.2
  362.5 1.3 copy-done.1
  363.8 5.4 fusion.5
  369.2 7.4 %add_convert_fusion = bf16[512,2048]{1,0:T(8,128)(2,1)} fusion(f32[512,2048]{1,0:T(8,128)S(1)} %fusion.5, bf16[512,1408]{1,0:T(8,128)(2,1)S(1)} %get-tuple-element.16, bf16[1408,2048]{1,0:T(8,128)(2,1)} %all-gather.12.cloned.1.call-done), kind=kOutput, calls=%fused_computation.3 | convolution fusion | flops 2954887168 | bytes 13500416 | tf_op jit(solution)/shard_map/dot_general | solution.py:29
  376.6 76.8 %reduce-scatter.11.cloned.1.call-done = bf16[1408,256]{1,0:T(8,128)(2,1)} async-done(((bf16[1408,2048]{1,0:T(8,128)(2,1)}), bf16[1408,256]{1,0:T(8,128)(2,1)}) %reduce-scatter.11.cloned.1.call-update) | async-done | bytes 720912 | tf_op jit(solution)/shard_map/reduce_scatter | solution.py:47
  453.5 2.3 multiply_reduce_fusion
  455.8 111.8 %reduce-scatter.9.cloned.1.call-done = bf16[1408,256]{1,0:T(8,128)(2,1)} async-done(((bf16[1408,2048]{1,0:T(8,128)(2,1)}), bf16[1408,256]{1,0:T(8,128)(2,1)}) %reduce-scatter.9.cloned.1.call-update) | async-done | bytes 720912 | tf_op jit(solution)/shard_map/reduce_scatter | solution.py:44
  567.6 2.3 multiply_reduce_fusion.1
  569.9 111.8 %reduce-scatter.7.cloned.1.call-done = bf16[1408,256]{1,0:T(8,128)(2,1)} async-done(((bf16[1408,2048]{1,0:T(8,128)(2,1)}), bf16[1408,256]{1,0:T(8,128)(2,1)}) %reduce-scatter.7.cloned.1.call-update) | async-done | bytes 720912 | tf_op jit(solution)/shard_map/reduce_scatter | solution.py:41
  681.7 2.3 multiply_reduce_fusion.2
  684.0 35.5 %all-reduce = (f32[1408]{0:T(1024)S(1)}, f32[1408]{0:T(1024)S(1)}, f32[1408]{0:T(1024)S(1)}) all-reduce(f32[1408]{0:T(1024)S(1)} %get-tuple-element.14, f32[1408]{0:T(1024)S(1)} %get-tuple-element.12, f32[1408]{0:T(1024)S(1)} %get-tuple-element.10), channel_id=1, replica_groups=mesh['fs'=8,'tp'=4] {'fs'}, use_global_device_ids=true, to_apply=%region_5.0 | all-reduce | flops 4224 | bytes 33792 | tf_op jit(solution)/shard_map/psum | solution.py:51
  (21 shorter events, 2.9 us)
Async XLA Ops:
  7.2 27.7 %all-gather.10.cloned.1.call-start = ((), (), s32[]{:S(2)}) async-start(), calls=%async_computation.6 | async-start | bytes 2621440 | tf_op jit(solution)/shard_map/all_gather | solution.py:10
  7.9 122.2 %all-gather.12.cloned.1.call-start = ((), (), s32[]{:S(2)}) async-start(), calls=%async_computation.7 | async-start | bytes 6488064 | tf_op jit(solution)/shard_map/all_gather | solution.py:15
  8.6 214.8 %all-gather.14.cloned.1.call-start = ((), (), s32[]{:S(2)}) async-start(), calls=%async_computation.8 | async-start | bytes 6488064 | tf_op jit(solution)/shard_map/all_gather | solution.py:14
  9.4 236.3 %all-gather.6.cloned.1.call-start = ((), (), s32[]{:S(2)}) async-start(), calls=%async_computation.4 | async-start | bytes 2621440 | tf_op jit(solution)/shard_map/all_gather | solution.py:11
  10.0 330.7 %all-gather.8.cloned.1.call-start = ((), (), s32[]{:S(2)}) async-start(), calls=%async_computation.5 | async-start | bytes 6488064 | tf_op jit(solution)/shard_map/all_gather | solution.py:16
  10.5 442.9 %reduce-scatter.11.cloned.1.call-start = ((), (), s32[]{:S(2)}) async-start(), calls=%async_computation.12 | async-start | bytes 6488064 | tf_op jit(solution)/shard_map/reduce_scatter | solution.py:47
  34.9 188.6 %copy-start = (bf16[512,2048]{1,0:T(8,128)(2,1)S(1)}, bf16[512,2048]{1,0:T(8,128)(2,1)}, u32[]{:S(2)}) copy-start(bf16[512,2048]{1,0:T(8,128)(2,1)} %all-gather.10.cloned.1.call-done) | copy-start | bytes 6291460
  254.7 312.8 %reduce-scatter.9.cloned.1.call-start = ((), (), s32[]{:S(2)}) async-start(), calls=%async_computation.11 | async-start | bytes 6488064 | tf_op jit(solution)/shard_map/reduce_scatter | solution.py:44
  355.9 325.8 %reduce-scatter.7.cloned.1.call-start = ((), (), s32[]{:S(2)}) async-start(), calls=%async_computation.10 | async-start | bytes 6488064 | tf_op jit(solution)/shard_map/reduce_scatter | solution.py:41
  362.4 1.4 copy-start.1
  362.4 358.3 %reduce-scatter.5.cloned.1.call-start = ((), (), s32[]{:S(2)}) async-start(), calls=%async_computation.9 | async-start | bytes 2621440 | tf_op jit(solution)/shard_map/reduce_scatter | solution.py:28
Sparse Core Ops, SparseCore 0:
  9.5 25.2 all-gather.9
  36.9 93.1 all-gather.11
  132.1 91.3 all-gather.13
  224.9 20.7 all-gather.5
  247.5 93.1 all-gather.7
  344.2 109.1 reduce-scatter.10
  457.1 110.3 reduce-scatter.8
  571.2 110.3 reduce-scatter.6
  684.8 30.5 reduce-scatter.4
where the time goes:
time: 728 us; the launch traced here: 727 us
  waiting for transfers between devices  608 us (84%)
  matrix products  59.5 us (8%)
  blocking collectives  35.5 us (5%)
  between operations  13.9 us (2%)
  other arithmetic  8.24 us (1%)
    reduce_scatter x1, waiting for transfers between devices, body(): lax.psum_scatter(part_up.astype(jnp.bfloat16), 'fs', scatter_dimension=1,...  112 us
    reduce_scatter x1, waiting for transfers between devices, body(): lax.psum_scatter(part_gate.astype(jnp.bfloat16), 'fs', scatter_dimension=...  112 us
    all_gather x1, waiting for transfers between devices, body(): lax.all_gather(up_weight, 'fs', axis=1, tiled=True)  95.2 us
    all_gather x1, waiting for transfers between devices, body(): lax.all_gather(down_weight, 'fs', axis=1, tiled=True)  85.7 us
    all_gather x1, waiting for transfers between devices, body(): lax.all_gather(gate_weight, 'fs', axis=1, tiled=True)  85.1 us
    reduce_scatter x1, waiting for transfers between devices, body(): lax.psum_scatter(part_down.astype(jnp.bfloat16), 'fs', scatter_dimension=...  76.8 us
    psum x1, blocking collectives, body(): lax.psum((jnp.sum(grad_gate * grad_gate, axis=1), jnp.sum(grad_up * grad_...  35.5 us
    all_gather x1, waiting for transfers between devices, body(): lax.all_gather(tokens, 'tp', axis=0, tiled=True)  24.3 us
  transfers between devices with their start and end apart: 9, of which 8 were waited for; matrix products, arithmetic and copies ran while one was open for 9% of the time, Pallas kernels for 0%

commit v1 on v0

--- a/solution.py
+++ b/solution.py
@@ -3,6 +3,18 @@
 import jax.numpy as jnp
 from jax import lax
 from jax.sharding import PartitionSpec as P
+
+
+def doubled_up(x, axis, dim):
+    ways, here, step = (lax.axis_size(axis), lax.axis_index(axis), x.shape[dim])
+    line, have = (x, 1)
+    while have < ways:
+        line = jnp.concatenate(
+            [line, lax.ppermute(line, axis, [(d, (d - have) % ways) for d in range(ways)])],
+            axis=dim,
+        )
+        have = 2 * have
+    return jnp.roll(line, here * step, axis=dim)
 
 
 def body(tokens, gate_weight, up_weight, down_weight, out_grad):
@@ -13,7 +25,7 @@
     w_gate, w_up, w_down = (
         lax.all_gather(gate_weight, "fs", axis=1, tiled=True),
         lax.all_gather(up_weight, "fs", axis=1, tiled=True),
-        lax.all_gather(down_weight, "fs", axis=1, tiled=True),
+        doubled_up(down_weight, "fs", 1),
     )
     inner = (((1,), (1,)), ((), ()))
     gate = lax.dot_general(inputs, w_gate, inner, preferred_element_type=jnp.float32)

time: 728 us -> 760 us (1.044)
  local copies, waits for them, and re-layouts: 1.29 us -> 17.2 us
  waiting for transfers between devices: 608 us -> 616 us
    ppermute x0 -> x3, waiting for transfers between devices: none -> 259 us  [doubled_up(): lax.ppermute(line, axis, [(d, (d - have) % ways) for d in range(ways)])]
    all_gather x1 -> x0, waiting for transfers between devices: 85.7 us -> none  [body(): lax.all_gather(down_weight, 'fs', axis=1, tiled=True)]
    all_gather x1, waiting for transfers between devices: 85.1 us -> 0.01 us  [body(): lax.all_gather(gate_weight, 'fs', axis=1, tiled=True)]
    all_gather x1, waiting for transfers between devices: 95.2 us -> 36.5 us  [body(): lax.all_gather(up_weight, 'fs', axis=1, tiled=True)]
    reduce_scatter x1, waiting for transfers between devices: 76.8 us -> 112 us  [body(): lax.psum_scatter(part_down.astype(jnp.bfloat16), 'fs', scatter_dimension=...]
    reduce_scatter x1, waiting for transfers between devices: 112 us -> 80.6 us  [body(): lax.psum_scatter(part_up.astype(jnp.bfloat16), 'fs', scatter_dimension=1,...]
    all_gather x1, waiting for transfers between devices: 24.3 us -> 0.01 us  [body(): lax.all_gather(tokens, 'tp', axis=0, tiled=True)]
    unnamed x4 -> x15, local copies, waits for them, and re-layouts: 1.29 us -> 13.4 us
  transfers between devices with their start and end apart: 9 -> 11, of which waited for: 8 -> 8; matrix products, arithmetic and copies ran while one was open for 9% -> 9% of each run, Pallas kernels for 0% -> 0%
where the time goes in v1:
time: 760 us
  waiting for transfers between devices  616 us (81%)
  matrix products  57.9 us (8%)
  blocking collectives  35.5 us (5%)
  local copies, waits for them, and re-layouts  17.2 us (2%)
  between operations  14.2 us (2%)
  other arithmetic  11.5 us (2%)
  starting transfers between devices  7.86 us (1%)
    ppermute x3, waiting for transfers between devices, doubled_up(): lax.ppermute(line, axis, [(d, (d - have) % ways) for d in range(ways)])  259 us
    reduce_scatter x1, waiting for transfers between devices, body(): lax.psum_scatter(part_down.astype(jnp.bfloat16), 'fs', scatter_dimension=...  112 us
    reduce_scatter x1, waiting for transfers between devices, body(): lax.psum_scatter(part_gate.astype(jnp.bfloat16), 'fs', scatter_dimension=...  112 us
    reduce_scatter x1, waiting for transfers between devices, body(): lax.psum_scatter(part_up.astype(jnp.bfloat16), 'fs', scatter_dimension=1,...  80.6 us
    all_gather x1, waiting for transfers between devices, body(): lax.all_gather(up_weight, 'fs', axis=1, tiled=True)  36.5 us
    psum x1, blocking collectives, body(): lax.psum((jnp.sum(grad_gate * grad_gate, axis=1), jnp.sum(grad_up * grad_...  35.5 us
  transfers between devices with their start and end apart: 11, of which 8 were waited for; matrix products, arithmetic and copies ran while one was open for 9% of the time, Pallas kernels for 0%

profile of v1, /device:TPU:0, one launch (start us, length us, event | category | flops | bytes accessed | tf_op | source)
XLA Modules:
  0.0 759.9 jit_solution(9355302498072230193)
XLA Ops:
  9.4 6.1 collective-permute-start
  15.5 15.7 %collective-permute-done = bf16[1408,256]{1,0:T(8,128)(2,1)S(1)} collective-permute-done((bf16[1408,256]{1,0:T(8,128)(2,1)}, bf16[1408,256]{1,0:T(8,128)(2,1)S(1)}, u32[]{:S(2)}, u32[]{:S(2)}) %collective-permute-start) | collective-permute-done | bytes 720928 | tf_op jit(solution)/shard_map/ppermute | solution.py:13
  33.9 52.2 %collective-permute-done.1 = bf16[1408,512]{1,0:T(8,128)(2,1)S(1)} collective-permute-done((bf16[1408,512]{1,0:T(8,128)(2,1)S(1)}, bf16[1408,512]{1,0:T(8,128)(2,1)S(1)}, u32[]{:S(2)}, u32[]{:S(2)}) %collective-permute-start.1) | collective-permute-done | bytes 1441824 | tf_op jit(solution)/shard_map/ppermute | solution.py:13
  86.2 2.0 pad_maximum_fusion
  91.4 190.6 %collective-permute-done.2 = bf16[1408,1024]{1,0:T(8,128)(2,1)} collective-permute-done((bf16[1408,1024]{1,0:T(8,128)(2,1)}, bf16[1408,1024]{1,0:T(8,128)(2,1)}, u32[]{:S(2)}, u32[]{:S(2)}) %collective-permute-start.2) | collective-permute-done | bytes 2883616 | tf_op jit(solution)/shard_map/ppermute | solution.py:13
  282.0 3.7 constant_dynamic-update-slice_fusion.4
  289.0 3.7 constant_dynamic-update-slice_fusion
  292.7 8.2 %fusion.10 = f32[512,1408]{0,1:T(8,128)} fusion(bf16[512,2048]{1,0:T(8,128)(2,1)} %all-gather.7.cloned.1.call-done, bf16[1408,2048]{1,0:T(8,128)(2,1)} %all-gather.11.cloned.1.call-done), kind=kOutput, calls=%fused_computation.31 | convolution fusion | flops 2952790016 | bytes 10747904 | tf_op jit(solution)/shard_map/dot_general | solution.py:31
  300.9 36.5 %all-gather.9.cloned.1.call-done = bf16[1408,2048]{1,0:T(8,128)(2,1)} async-done(((bf16[1408,256]{1,0:T(8,128)(2,1)}), bf16[1408,2048]{1,0:T(8,128)(2,1)}) %all-gather.9.cloned.1.call-update) | async-done | bytes 5767184 | tf_op jit(solution)/shard_map/all_gather | solution.py:27
  337.4 7.4 fusion.9
  344.8 14.8 %all-gather.5.cloned.1.call-done = bf16[512,2048]{1,0:T(8,128)(2,1)} async-done(((bf16[128,2048]{1,0:T(8,128)(2,1)}), bf16[512,2048]{1,0:T(8,128)(2,1)}) %all-gather.5.cloned.1.call-update) | async-done | bytes 2097168 | tf_op jit(solution)/shard_map/all_gather | solution.py:23
  359.6 10.2 %multiply_convert_fusion.4 = (bf16[512,1408]{0,1:T(8,128)(2,1)S(1)}, bf16[512,1408]{0,1:T(8,128)(2,1)}) fusion(f32[512,1408]{0,1:T(8,128)} %fusion.10, f32[512,1408]{0,1:T(8,128)} %fusion.9, bf16[512,2048]{1,0:T(8,128)(2,1)} %all-gather.5.cloned.1.call-done, bf16[1408,4096]{1,0:T(8,128)(2,1)} %constant_dynamic-update-slice_fusion, s32[]{:T(128)S(6)} %select_n.14), kind=kOutput, calls=%fused_computation.9 | convolution fusion | flops 2962161664 | bytes 16515076 | tf_op jit(solution)/shard_map/dot_general | solution.py:33
  369.9 5.0 multiply_convert_fusion.1
  374.9 6.4 multiply_convert_fusion.2
  383.3 7.9 %multiply_convert_fusion = bf16[1408,2048]{1,0:T(8,128)(2,1)} fusion(bf16[512,2048]{1,0:T(8,128)(2,1)S(1)} %copy-done.2, f32[512,1408]{0,1:T(8,128)} %fusion.9, f32[512,1408]{0,1:T(8,128)} %fusion.10), kind=kOutput, calls=%fused_computation | convolution fusion | flops 2962882560 | bytes 13631488 | tf_op jit(solution)/shard_map/dot_general | solution.py:51
  392.6 5.5 fusion.11
  398.0 7.4 add_convert_fusion
  405.4 80.6 %reduce-scatter.9.cloned.1.call-done = bf16[1408,256]{1,0:T(8,128)(2,1)} async-done(((bf16[1408,2048]{1,0:T(8,128)(2,1)}), bf16[1408,256]{1,0:T(8,128)(2,1)}) %reduce-scatter.9.cloned.1.call-update) | async-done | bytes 720912 | tf_op jit(solution)/shard_map/reduce_scatter | solution.py:56
  486.0 2.3 multiply_reduce_fusion.1
  488.4 111.6 %reduce-scatter.7.cloned.1.call-done = bf16[1408,256]{1,0:T(8,128)(2,1)} async-done(((bf16[1408,2048]{1,0:T(8,128)(2,1)}), bf16[1408,256]{1,0:T(8,128)(2,1)}) %reduce-scatter.7.cloned.1.call-update) | async-done | bytes 720912 | tf_op jit(solution)/shard_map/reduce_scatter | solution.py:53
  600.0 2.3 multiply_reduce_fusion.2
  602.3 111.7 %reduce-scatter.11.cloned.1.call-done = bf16[1408,256]{1,0:T(8,128)(2,1)} async-done(((bf16[1408,2048]{1,0:T(8,128)(2,1)}), bf16[1408,256]{1,0:T(8,128)(2,1)}) %reduce-scatter.11.cloned.1.call-update) | async-done | bytes 720912 | tf_op jit(solution)/shard_map/reduce_scatter | solution.py:59
  714.0 2.3 multiply_reduce_fusion
  716.4 35.5 %all-reduce = (f32[1408]{0:T(1024)S(1)}, f32[1408]{0:T(1024)S(1)}, f32[1408]{0:T(1024)S(1)}) all-reduce(f32[1408]{0:T(1024)S(1)} %get-tuple-element.14, f32[1408]{0:T(1024)S(1)} %get-tuple-element.12, f32[1408]{0:T(1024)S(1)} %get-tuple-element.10), channel_id=1, replica_groups=mesh['fs'=8,'tp'=4] {'fs'}, use_global_device_ids=true, to_apply=%region_5.6 | all-reduce | flops 4224 | bytes 33792 | tf_op jit(solution)/shard_map/psum | solution.py:63
  (38 shorter events, 16.1 us)
Async XLA Ops:
  7.2 79.0 %copy-start = (bf16[1408,256]{1,0:T(8,128)(2,1)S(1)}, bf16[1408,256]{1,0:T(8,128)(2,1)}, u32[]{:S(2)}) copy-start(bf16[1408,256]{1,0:T(8,128)(2,1)} %param.8) | copy-start | bytes 2162692
  7.2 285.5 %all-gather.7.cloned.1.call-start = ((), (), s32[]{:S(2)}) async-start(), calls=%async_computation.5 | async-start | bytes 2621440 | tf_op jit(solution)/shard_map/all_gather | solution.py:22
  7.9 284.8 %all-gather.11.cloned.1.call-start = ((), (), s32[]{:S(2)}) async-start(), calls=%async_computation.7 | async-start | bytes 6488064 | tf_op jit(solution)/shard_map/all_gather | solution.py:26
  8.7 328.8 %all-gather.9.cloned.1.call-start = ((), (), s32[]{:S(2)}) async-start(), calls=%async_computation.6 | async-start | bytes 6488064 | tf_op jit(solution)/shard_map/all_gather | solution.py:27
  9.4 350.2 %all-gather.5.cloned.1.call-start = ((), (), s32[]{:S(2)}) async-start(), calls=%async_computation.4 | async-start | bytes 2621440 | tf_op jit(solution)/shard_map/all_gather | solution.py:23
  9.4 21.8 %collective-permute-start = (bf16[1408,256]{1,0:T(8,128)(2,1)}, bf16[1408,256]{1,0:T(8,128)(2,1)S(1)}, u32[]{:S(2)}, u32[]{:S(2)}) collective-permute-start(bf16[1408,256]{1,0:T(8,128)(2,1)} %param.8), channel_id=1, source_target_pairs={{0,28},{4,0},{8,4},{12,8},{16,12},{20,16},{24,20},{28,24},{1,29},{... | collective-permute-start | bytes 2162696 | tf_op jit(solution)/shard_map/ppermute | solution.py:13
  32.5 53.7 %collective-permute-start.1 = (bf16[1408,512]{1,0:T(8,128)(2,1)S(1)}, bf16[1408,512]{1,0:T(8,128)(2,1)S(1)}, u32[]{:S(2)}, u32[]{:S(2)}) collective-permute-start(bf16[1408,512]{1,0:T(8,128)(2,1)S(1)} %pad_maximum_fusion.1), channel_id=1, source_target_pairs={{0,24},{4,28},{8,0},{12,4},{16,8},{20,12},{24,16},{28,20},{1,25},{... | collective-permute-start | bytes 4325384 | tf_op jit(solution)/shard_map/ppermute | solution.py:13
  88.1 193.9 %collective-permute-start.2 = (bf16[1408,1024]{1,0:T(8,128)(2,1)}, bf16[1408,1024]{1,0:T(8,128)(2,1)}, u32[]{:S(2)}, u32[]{:S(2)}) collective-permute-start(bf16[1408,1024]{1,0:T(8,128)(2,1)} %pad_maximum_fusion), channel_id=1, source_target_pairs={{0,16},{4,20},{8,24},{12,28},{16,0},{20,4},{24,8},{28,12},{1,17},{... | collective-permute-start | bytes 8650760 | tf_op jit(solution)/shard_map/ppermute | solution.py:13
  88.2 397.9 %reduce-scatter.9.cloned.1.call-start = ((), (), s32[]{:S(2)}) async-start(), calls=%async_computation.10 | async-start | bytes 6488064 | tf_op jit(solution)/shard_map/reduce_scatter | solution.py:56
  292.7 44.7 %copy-start.1 = (bf16[512,2048]{1,0:T(8,128)(2,1)S(1)}, bf16[512,2048]{1,0:T(8,128)(2,1)}, u32[]{:S(2)}) copy-start(bf16[512,2048]{1,0:T(8,128)(2,1)} %all-gather.7.cloned.1.call-done) | copy-start | bytes 6291460
  374.8 225.1 %reduce-scatter.7.cloned.1.call-start = ((), (), s32[]{:S(2)}) async-start(), calls=%async_computation.9 | async-start | bytes 6488064 | tf_op jit(solution)/shard_map/reduce_scatter | solution.py:53
  381.3 2.0 copy-start.2
  381.3 332.7 %reduce-scatter.11.cloned.1.call-start = ((), (), s32[]{:S(2)}) async-start(), calls=%async_computation.11 | async-start | bytes 6488064 | tf_op jit(solution)/shard_map/reduce_scatter | solution.py:59
  391.2 1.4 copy-start.3
  391.2 361.8 %reduce-scatter.5.cloned.1.call-start = ((), (), s32[]{:S(2)}) async-start(), calls=%async_computation.8 | async-start | bytes 2621440 | tf_op jit(solution)/shard_map/reduce_scatter | solution.py:40
Sparse Core Ops, SparseCore 0:
  9.5 25.2 all-gather.6
  36.9 195.9 all-gather.10
  235.0 102.4 all-gather.8
  338.8 20.7 all-gather.4
  375.0 111.0 reduce-scatter.8
  489.5 110.3 reduce-scatter.6
  603.6 110.3 reduce-scatter.10
  717.1 30.4 reduce-scatter.4
